TPU v7x, 512 devices: a whole 4x8x8 slice. The times are simulated.
512 devices in a mesh: row: 64 (over z, y), col: 8 (over x, core).
Axes of the slice: x: 4, y: 8, z: 8, core: 2. Of those that a mesh axis runs over, the one named last changes fastest.
Arguments:
- tokens: bfloat16 [8, 24576, 2048], P('col', 'row'), may hold values from -6 to 6
- norm_gain: bfloat16 [2048], replicated, may hold values from 0.099609375 to 1.8984375
- in_weight: bfloat16 [2048, 512], P('row', 'col'), may hold values from -0.125 to 0.125
- out_weight: bfloat16 [512, 2048], P('col', 'row'), may hold values from -0.25 to 0.25
Outputs:
- mixed: bfloat16 [8, 24576, 2048], P('col', 'row')
All inputs are finite; a program needn't handle non-finite values.
Results may differ from a plain program's by a relative error of at most 0.013.
Values may be sent and summed in bfloat16 or wider, within the bound.
A program may use at most 64 MiB of HBM per device.

v0:
```python
import math
import jax
import jax.numpy as jnp
from jax import lax
from jax.sharding import Mesh
from jax.sharding import PartitionSpec as P

GS = 64
ROW = ("row_0", "row_1")
EPS = 1e-06


def turned_gather(arrays, axis, dims):
    turned = [jnp.moveaxis(a, dim, 0) for a, dim in zip(arrays, dims)]
    widths = [t[0].size for t in turned]
    both = jnp.concatenate([t.reshape(-1, w) for t, w in zip(turned, widths)], axis=1)
    out = lax.all_gather(both, axis, axis=0, tiled=True)
    pieces = jnp.split(out, [sum(widths[:k]) for k in range(1, len(widths))], axis=1)
    return tuple(
        (
            jnp.moveaxis(b.reshape(-1, *t.shape[1:]), 0, dim)
            for b, t, dim in zip(pieces, turned, dims)
        )
    )


def joined_along(pieces, dim):
    pieces = jnp.moveaxis(pieces, 0, dim)
    lengths = pieces.shape
    return pieces.reshape(*lengths[:dim], lengths[dim] * lengths[dim + 1], *lengths[dim + 2 :])


def all_blocks(shard, axes, sequence):
    pieces = shard
    for k in sequence:
        pieces = lax.all_gather(pieces, axes[k])
    done = sequence[::-1]
    back = [done.index(k) for k in range(len(axes))]
    pieces = pieces.transpose(*back, *range(len(axes), pieces.ndim))
    return pieces.reshape(-1, *shard.shape)


def gather_axes(shard, axes, sequence, dim):
    return joined_along(all_blocks(shard, axes, sequence), dim)


def angle_pair(left_index, right_index, modulus):
    product = left_index[:, None] * right_index[None, :] % modulus
    radians = product.astype(jnp.float32) * (2.0 * math.pi / modulus)
    return (jnp.cos(radians), jnp.sin(radians))


def table_dot(matrix, values):
    return jnp.dot(matrix, values, preferred_element_type=jnp.float32)


def right_dot(values, matrix):
    return jnp.dot(values, matrix, preferred_element_type=jnp.float32)


def body(tokens, norm_gain, in_weight, out_weight):
    own_rows = tokens[0].astype(jnp.float32)
    inverse_rms = lax.rsqrt(jnp.mean(own_rows * own_rows, axis=-1, keepdims=True) + EPS)
    normed = (own_rows * inverse_rms * norm_gain.astype(jnp.float32)).astype(jnp.bfloat16)
    in_columns, out_rows = turned_gather((in_weight, out_weight), "col", (1, 0))
    row_count = normed.shape[0]
    channels = in_columns.shape[1]
    peer_count = lax.axis_size(ROW)
    length = row_count * peer_count
    projected = jnp.dot(
        normed, gather_axes(in_columns, ROW, (0, 1), 0), preferred_element_type=jnp.float32
    ).astype(jnp.bfloat16)
    channel_index = jnp.arange(channels, dtype=jnp.int32)
    within = channel_index % GS
    same_group = channel_index[:, None] // GS == channel_index[None, :] // GS
    group_cos, group_sin = angle_pair(within, within, GS)
    group_cos = jnp.where(same_group, group_cos, 0.0)
    group_sin = jnp.where(same_group, group_sin, 0.0)
    peer_index = jnp.arange(peer_count, dtype=jnp.int32)
    small_cos, small_sin = angle_pair(peer_index, peer_index, peer_count)
    line_index = jnp.arange(row_count, dtype=jnp.int32)
    long_cos, long_sin = angle_pair(line_index, line_index, row_count)
    gathered = lax.all_to_all(projected, ROW, split_axis=1, concat_axis=0, tiled=True).astype(
        jnp.float32
    )
    narrow = gathered.shape[1]
    flat = gathered.reshape(peer_count, row_count * narrow)
    first_real = table_dot(small_cos, flat).reshape(peer_count, row_count, narrow)
    first_imag = (-table_dot(small_sin, flat)).reshape(peer_count, row_count, narrow)
    turn_cos, turn_sin = angle_pair(peer_index, line_index, length)
    turn_cos = turn_cos[:, :, None]
    turn_sin = turn_sin[:, :, None]
    turned_real = first_real * turn_cos + first_imag * turn_sin
    turned_imag = first_imag * turn_cos - first_real * turn_sin
    lines_real = turned_real.transpose(1, 0, 2).reshape(row_count, peer_count * narrow)
    lines_imag = turned_imag.transpose(1, 0, 2).reshape(row_count, peer_count * narrow)
    whole_real = (table_dot(long_cos, lines_real) + table_dot(long_sin, lines_imag)).reshape(
        length, narrow
    )
    whole_imag = (table_dot(long_cos, lines_imag) - table_dot(long_sin, lines_real)).reshape(
        length, narrow
    )
    back_real, back_imag = (
        lax.all_to_all(
            whole_real.astype(jnp.bfloat16), ROW, split_axis=0, concat_axis=1, tiled=True
        ).astype(whole_real.dtype),
        lax.all_to_all(
            whole_imag.astype(jnp.bfloat16), ROW, split_axis=0, concat_axis=1, tiled=True
        ).astype(whole_imag.dtype),
    )
    mixed_real = right_dot(back_real, group_cos) + right_dot(back_imag, group_sin)
    arranged = (mixed_real * (1.0 / math.sqrt(length * GS))).astype(jnp.bfloat16)
    result = jnp.dot(
        arranged,
        lax.all_gather(out_rows, ROW, axis=1, tiled=True),
        preferred_element_type=jnp.float32,
    )
    return result.astype(jnp.bfloat16)[None]


def solution(mesh):
    split = Mesh(mesh.devices.reshape(8, 8, mesh.shape["col"]), ("row_0", "row_1", "col"))
    in_specs = (P("col", ROW, None), P(), P(ROW, "col"), P("col", ROW))
    out_specs = P("col", ROW, None)
    return jax.shard_map(body, mesh=split, in_specs=in_specs, out_specs=out_specs, check_vma=False)
```

profile of v0, /device:TPU:2, one launch (start us, length us, event | category | flops | bytes accessed | tf_op | source)
XLA Modules:
  0.0 213.6 jit_solution(14317200805764714633)
XLA Ops:
  6.5 0.9 copy.54
  7.4 0.8 copy.55
  8.3 15.4 %all_gather.18 = bf16[512,64]{1,0:T(8,128)(2,1)S(1)} all-gather(bf16[64,64]{1,0:T(8,128)(2,1)S(1)} %pad_maximum_fusion), channel_id=1, replica_groups=mesh['row_0'=8,'row_1'=8,'col'=8] {'col'}, dimensions={0}, use_global_device_ids=true | all-gather | bytes 73728 | tf_op jit(solution)/shard_map/all_gather | solution.py:17
  24.0 30.5 %all-gather = bf16[256,512]{1,0:T(8,128)(2,1)} all-gather(bf16[32,512]{1,0:T(8,128)(2,1)S(1)} %bitcast.62), channel_id=2, replica_groups=mesh['row_0'=8,'row_1'=8,'col'=8] {'row_0'}, dimensions={0}, use_global_device_ids=true | all-gather | bytes 294912 | tf_op jit(solution)/shard_map/all_gather | solution.py:36
  54.5 0.7 copy.68
  55.3 0.7 convert_element_type.78
  56.0 0.4 fusion
  56.3 39.7 %all-gather.7.cloned.1.call-done = bf16[64,32,512]{2,1,0:T(8,128)(2,1)} async-done(((bf16[8,32,512]{2,1,0:T(8,128)(2,1)}), bf16[64,32,512]{2,1,0:T(8,128)(2,1)}) %all-gather.7.cloned.1.call-update) | async-done | bytes 2097168 | tf_op jit(solution)/shard_map/all_gather | solution.py:36
  96.0 1.8 copy.57
  97.9 1.0 fusion.13
  98.9 0.9 copy.58
  99.8 10.7 %all-to-all-start = ((bf16[384,64,8]{0,2,1:T(8,128)(2,1)}), bf16[384,64,8]{0,2,1:T(8,128)(2,1)S(1)}, u32[]{:S(2)}, u32[]{:S(2)}) async-start(bf16[384,64,8]{0,2,1:T(8,128)(2,1)} %bitcast.8), calls=%async_computation | async-start | bytes 786432 | tf_op jit(solution)/shard_map/all_to_all | solution.py:83
  110.6 0.4 fusion.78
  111.0 14.1 %all-to-all-done = bf16[384,64,8]{0,2,1:T(8,128)(2,1)S(1)} async-done(((bf16[384,64,8]{0,2,1:T(8,128)(2,1)}), bf16[384,64,8]{0,2,1:T(8,128)(2,1)S(1)}, u32[]{:S(2)}, u32[]{:S(2)}) %all-to-all-start) | async-done | bytes 393248 | tf_op jit(solution)/shard_map/all_to_all | solution.py:83
  125.1 0.6 copy.59
  125.7 0.5 convolution_negate_fusion
  126.2 0.5 copy.61
  126.7 0.5 copy.62
  127.2 0.5 subtract_bitcast_fusion
  127.7 2.5 %fusion.26 = f32[384,512]{1,0:T(8,128)S(1)} fusion(bf16[384,64,8]{0,1,2:T(8,128)(2,1)S(1)} %get-tuple-element.6), kind=kOutput, calls=%fused_computation.38 | convolution fusion | flops 152322048 | bytes 1179648 | tf_op jit(solution)/shard_map/dot_general | solution.py:54
  130.2 2.9 %fusion.10 = bf16[384,512]{1,0:T(8,128)(2,1)S(1)} fusion(f32[384,512]{1,0:T(8,128)S(1)} %fusion.26, bf16[384,64,8]{0,1,2:T(8,128)(2,1)S(1)} %get-tuple-element.5), kind=kOutput, calls=%fused_computation.23 | convolution fusion | flops 152715264 | bytes 1572864 | tf_op jit(solution)/shard_map/dot_general | solution.py:54
  133.1 8.4 %convert_element_type.84 = bf16[64,384,8]{2,1,0:T(8,128)(2,1)} reshape(bf16[384,512]{1,0:T(8,128)(2,1)S(1)} %fusion.10) | data formatting | bytes 786432 | tf_op jit(solution)/shard_map/convert_element_type | solution.py:105
  141.5 5.8 %copy.66 = bf16[64,384,8]{1,2,0:T(8,128)(2,1)} copy(bf16[64,384,8]{2,1,0:T(8,128)(2,1)} %convert_element_type.84) | data formatting | bytes 786432 | tf_op jit(solution)/shard_map/convert_element_type | solution.py:105
  147.3 4.8 %all-to-all-start.1 = ((bf16[64,384,8]{1,2,0:T(8,128)(2,1)}), bf16[64,384,8]{1,2,0:T(8,128)(2,1)S(1)}, u32[]{:S(2)}, u32[]{:S(2)}) async-start(bf16[64,384,8]{1,2,0:T(8,128)(2,1)} %copy.66), calls=%async_computation.1 | async-start | bytes 786432 | tf_op jit(solution)/shard_map/all_to_all | solution.py:104
  152.1 2.5 %fusion.22 = f32[384,512]{1,0:T(8,128)S(1)} fusion(bf16[384,64,8]{0,1,2:T(8,128)(2,1)S(1)} %get-tuple-element.5), kind=kOutput, calls=%fused_computation.34 | convolution fusion | flops 152322048 | bytes 1179648 | tf_op jit(solution)/shard_map/dot_general | solution.py:54
  154.6 2.9 %fusion.11 = bf16[384,512]{1,0:T(8,128)(2,1)S(1)} fusion(f32[384,512]{1,0:T(8,128)S(1)} %fusion.22, bf16[384,64,8]{0,1,2:T(8,128)(2,1)S(1)} %get-tuple-element.6), kind=kOutput, calls=%fused_computation.24 | convolution fusion | flops 152715264 | bytes 1572864 | tf_op jit(solution)/shard_map/dot_general | solution.py:54
  157.5 8.4 %convert_element_type.87 = bf16[64,384,8]{2,1,0:T(8,128)(2,1)} reshape(bf16[384,512]{1,0:T(8,128)(2,1)S(1)} %fusion.11) | data formatting | bytes 786432 | tf_op jit(solution)/shard_map/convert_element_type | solution.py:108
  165.9 5.8 %copy.67 = bf16[64,384,8]{1,2,0:T(8,128)(2,1)} copy(bf16[64,384,8]{2,1,0:T(8,128)(2,1)} %convert_element_type.87) | data formatting | bytes 786432 | tf_op jit(solution)/shard_map/convert_element_type | solution.py:108
  171.7 12.9 %all-to-all-start.2 = ((bf16[64,384,8]{1,2,0:T(8,128)(2,1)}), bf16[64,384,8]{1,2,0:T(8,128)(2,1)S(1)}, u32[]{:S(2)}, u32[]{:S(2)}) async-start(bf16[64,384,8]{1,2,0:T(8,128)(2,1)} %copy.67), calls=%async_computation.2 | async-start | bytes 786432 | tf_op jit(solution)/shard_map/all_to_all | solution.py:107
  184.7 4.2 %fusion.16 = f32[384,512]{1,0:T(8,128)S(1)} fusion(s32[512]{0:T(512)S(1)} %get-tuple-element.11, s32[512]{0:T(512)S(1)} %get-tuple-element.12, bf16[64,384,8]{1,2,0:T(8,128)(2,1)S(1)} %all-to-all-done.1), kind=kOutput, calls=%fused_computation.27 | convolution fusion | flops 205520896 | bytes 1183744 | tf_op jit(solution)/shard_map/dot_general | solution.py:58
  188.9 10.1 %all-to-all-done.2 = bf16[64,384,8]{1,2,0:T(8,128)(2,1)S(1)} async-done(((bf16[64,384,8]{1,2,0:T(8,128)(2,1)}), bf16[64,384,8]{1,2,0:T(8,128)(2,1)S(1)}, u32[]{:S(2)}, u32[]{:S(2)}) %all-to-all-start.2) | async-done | bytes 393248 | tf_op jit(solution)/shard_map/all_to_all | solution.py:107
  199.0 7.8 %fusion.3 = bf16[1,384,2048]{2,1,0:T(8,128)(2,1)} fusion(bf16[512,2048]{0,1:T(8,128)(2,1)} %all-gather.5.cloned.1.call-done, f32[384,512]{1,0:T(8,128)S(1)} %fusion.16, s32[512]{0:T(512)S(1)} %get-tuple-element.11, s32[512]{0:T(512)S(1)} %get-tuple-element.12, bf16[64,384,8]{1,2,0:T(8,128)(2,1)S(1)} %all-to-all-done.2), kind=kOutput, calls=%fused_computation.7 | convolution fusion | flops 1012203520 | bytes 4853760 | tf_op jit(solution)/shard_map/dot_general | solution.py:113
  (13 shorter events, 0.4 us)
Async XLA Ops:
  6.5 49.4 %copy-start = (bf16[1,384,2048]{2,1,0:T(8,128)(2,1)S(1)}, bf16[1,384,2048]{2,1,0:T(8,128)(2,1)}, u32[]{:S(2)}) copy-start(bf16[1,384,2048]{2,1,0:T(8,128)(2,1)} %param.4) | copy-start | bytes 4718596
  6.5 89.5 %all-gather.7.cloned.1.call-start = ((), (), s32[]{:S(2)}) async-start(), calls=%async_computation.4 | async-start | bytes 2359296 | tf_op jit(solution)/shard_map/all_gather | solution.py:36
  54.5 134.4 %all-gather.5.cloned.1.call-start = ((), (), s32[]{:S(2)}) async-start(), calls=%async_computation.3 | async-start | bytes 2129920 | tf_op jit(solution)/shard_map/all_gather | solution.py:115
  99.8 25.3 %all-to-all-start = ((bf16[384,64,8]{0,2,1:T(8,128)(2,1)}), bf16[384,64,8]{0,2,1:T(8,128)(2,1)S(1)}, u32[]{:S(2)}, u32[]{:S(2)}) async-start(bf16[384,64,8]{0,2,1:T(8,128)(2,1)} %bitcast.8), calls=%async_computation | async-start | bytes 786432 | tf_op jit(solution)/shard_map/all_to_all | solution.py:83
  147.3 24.4 %all-to-all-start.1 = ((bf16[64,384,8]{1,2,0:T(8,128)(2,1)}), bf16[64,384,8]{1,2,0:T(8,128)(2,1)S(1)}, u32[]{:S(2)}, u32[]{:S(2)}) async-start(bf16[64,384,8]{1,2,0:T(8,128)(2,1)} %copy.66), calls=%async_computation.1 | async-start | bytes 786432 | tf_op jit(solution)/shard_map/all_to_all | solution.py:104
  171.7 27.3 %all-to-all-start.2 = ((bf16[64,384,8]{1,2,0:T(8,128)(2,1)}), bf16[64,384,8]{1,2,0:T(8,128)(2,1)S(1)}, u32[]{:S(2)}, u32[]{:S(2)}) async-start(bf16[64,384,8]{1,2,0:T(8,128)(2,1)} %copy.67), calls=%async_computation.2 | async-start | bytes 786432 | tf_op jit(solution)/shard_map/all_to_all | solution.py:107
Sparse Core Ops, SparseCore 0:
  54.6 41.3 all-gather.6
  99.1 85.8 all-gather.4
where the time goes:
time: 214 us
  waiting for transfers between devices  64 us (30%)
  blocking collectives  45.9 us (21%)
  local copies, waits for them, and re-layouts  35.3 us (16%)
  starting transfers between devices  28.5 us (13%)
  matrix products  24.7 us (12%)
  between operations  13.5 us (6%)
    all_gather x1, waiting for transfers between devices, all_blocks(): pieces = lax.all_gather(pieces, axes[k])  39.7 us
    all_gather x1, blocking collectives, all_blocks(): pieces = lax.all_gather(pieces, axes[k])  30.5 us
    all_gather x1, blocking collectives, turned_gather(): out = lax.all_gather(both, axis, axis=0, tiled=True)  15.4 us
    convert_element_type x2, local copies, waits for them, and re-layouts, body(): whole_imag.astype(jnp.bfloat16)  14.2 us
    convert_element_type x2, local copies, waits for them, and re-layouts, body(): whole_real.astype(jnp.bfloat16)  14.2 us
    all_to_all x1, waiting for transfers between devices, body(): lax.all_to_all(projected, ROW, split_axis=1, concat_axis=0, tiled=True)  14.1 us
    all_to_all x1, starting transfers between devices, body(): lax.all_to_all(whole_imag.astype(jnp.bfloat16), ROW, split_axis=0, concat...  12.9 us
    dot_general x6, matrix products, table_dot(): return jnp.dot(matrix, values, preferred_element_type=jnp.float32)  11.7 us
  transfers between devices with their start and end apart: 5, of which 3 were waited for; matrix products, arithmetic and copies ran while one was open for 24% of the time, Pallas kernels for 0%

commit v1 on v0

--- a/solution.py
+++ b/solution.py
@@ -10,11 +10,16 @@
 EPS = 1e-06
 
 
+def exchange_gather(x, mesh_axis, d):
+    sent = jnp.stack([x] * lax.axis_size(mesh_axis))
+    return jnp.concatenate(lax.all_to_all(sent, mesh_axis, 0, 0), axis=d)
+
+
 def turned_gather(arrays, axis, dims):
     turned = [jnp.moveaxis(a, dim, 0) for a, dim in zip(arrays, dims)]
     widths = [t[0].size for t in turned]
     both = jnp.concatenate([t.reshape(-1, w) for t, w in zip(turned, widths)], axis=1)
-    out = lax.all_gather(both, axis, axis=0, tiled=True)
+    out = exchange_gather(both, axis, 0)
     pieces = jnp.split(out, [sum(widths[:k]) for k in range(1, len(widths))], axis=1)
     return tuple(
         (

time: 214 us -> 210 us (0.981)
  blocking collectives: 45.9 us -> 42 us
    all_gather x1 -> x0, blocking collectives: 15.4 us -> none  [turned_gather(): out = lax.all_gather(both, axis, axis=0, tiled=True)]
    all_to_all x0 -> x1, blocking collectives: none -> 12.4 us  [exchange_gather(): return jnp.concatenate(lax.all_to_all(sent, mesh_axis, 0, 0), axis=d)]
  transfers between devices with their start and end apart: 5 -> 5, of which waited for: 3 -> 3; matrix products, arithmetic and copies ran while one was open for 24% -> 25% of each run, Pallas kernels for 0% -> 0%
where the time goes in v1:
time: 210 us; the launch traced here: 209 us
  waiting for transfers between devices  64.2 us (31%)
  blocking collectives  42 us (20%)
  local copies, waits for them, and re-layouts  33.9 us (16%)
  starting transfers between devices  28.3 us (13%)
  matrix products  24.7 us (12%)
  between operations  13.5 us (6%)
  other arithmetic  2.34 us (1%)
    all_gather x1, waiting for transfers between devices, all_blocks(): pieces = lax.all_gather(pieces, axes[k])  39.6 us
    all_gather x1, blocking collectives, all_blocks(): pieces = lax.all_gather(pieces, axes[k])  29.6 us
    convert_element_type x2, local copies, waits for them, and re-layouts, body(): whole_imag.astype(jnp.bfloat16)  14.2 us
    convert_element_type x2, local copies, waits for them, and re-layouts, body(): whole_real.astype(jnp.bfloat16)  14.2 us
    all_to_all x1, waiting for transfers between devices, body(): lax.all_to_all(projected, ROW, split_axis=1, concat_axis=0, tiled=True)  14.1 us
    all_to_all x1, starting transfers between devices, body(): lax.all_to_all(whole_imag.astype(jnp.bfloat16), ROW, split_axis=0, concat...  12.7 us
    all_to_all x1, blocking collectives, exchange_gather(): return jnp.concatenate(lax.all_to_all(sent, mesh_axis, 0, 0), axis=d)  12.4 us
    dot_general x6, matrix products, table_dot(): return jnp.dot(matrix, values, preferred_element_type=jnp.float32)  11.7 us
  transfers between devices with their start and end apart: 5, of which 3 were waited for; matrix products, arithmetic and copies ran while one was open for 25% of the time, Pallas kernels for 0%

profile of v1, /device:TPU:2, one launch (start us, length us, event | category | flops | bytes accessed | tf_op | source)
XLA Modules:
  0.0 208.9 jit_solution(13310759961792153163)
XLA Ops:
  6.5 0.8 pad_maximum_fusion
  7.4 0.2 reshape.191
  7.6 12.4 %all_to_all.53 = bf16[8,2,2048]{2,1,0:T(2,128)(2,1)S(1)} all-to-all(bf16[8,2,2048]{2,1,0:T(2,128)(2,1)S(1)} %reshape.191), channel_id=1, replica_groups=mesh['row_0'=8,'row_1'=8,'col'=8] {'col'}, dimensions={0} | all-to-all | bytes 131072 | tf_op jit(solution)/shard_map/all_to_all | solution.py:15
  20.4 0.6 slice_bitcast_fusion
  21.0 29.6 %all-gather = bf16[256,512]{1,0:T(8,128)(2,1)} all-gather(bf16[32,512]{1,0:T(8,128)(2,1)S(1)} %get-tuple-element.7), channel_id=2, replica_groups=mesh['row_0'=8,'row_1'=8,'col'=8] {'row_0'}, dimensions={0}, use_global_device_ids=true | all-gather | bytes 294912 | tf_op jit(solution)/shard_map/all_gather | solution.py:41
  50.6 0.7 convert_element_type.78
  51.3 0.4 fusion
  51.7 39.6 %all-gather.7.cloned.1.call-done = bf16[64,32,512]{2,1,0:T(8,128)(2,1)} async-done(((bf16[8,32,512]{2,1,0:T(8,128)(2,1)}), bf16[64,32,512]{2,1,0:T(8,128)(2,1)}) %all-gather.7.cloned.1.call-update) | async-done | bytes 2097168 | tf_op jit(solution)/shard_map/all_gather | solution.py:41
  91.4 1.8 copy.29
  93.2 1.0 fusion.13
  94.2 0.9 copy.30
  95.2 10.7 %all-to-all-start.1 = ((bf16[384,64,8]{0,2,1:T(8,128)(2,1)}), bf16[384,64,8]{0,2,1:T(8,128)(2,1)S(1)}, u32[]{:S(2)}, u32[]{:S(2)}) async-start(bf16[384,64,8]{0,2,1:T(8,128)(2,1)} %bitcast.8), calls=%async_computation.1 | async-start | bytes 786432 | tf_op jit(solution)/shard_map/all_to_all | solution.py:88
  105.9 0.4 fusion.78
  106.3 14.1 %all-to-all-done.1 = bf16[384,64,8]{0,2,1:T(8,128)(2,1)S(1)} async-done(((bf16[384,64,8]{0,2,1:T(8,128)(2,1)}), bf16[384,64,8]{0,2,1:T(8,128)(2,1)S(1)}, u32[]{:S(2)}, u32[]{:S(2)}) %all-to-all-start.1) | async-done | bytes 393248 | tf_op jit(solution)/shard_map/all_to_all | solution.py:88
  120.4 0.6 copy.31
  121.1 0.5 convolution_negate_fusion
  121.5 0.5 copy.33
  122.0 0.5 copy.34
  122.6 0.5 subtract_bitcast_fusion
  123.0 2.5 %fusion.26 = f32[384,512]{1,0:T(8,128)S(1)} fusion(bf16[384,64,8]{0,1,2:T(8,128)(2,1)S(1)} %get-tuple-element.6), kind=kOutput, calls=%fused_computation.38 | convolution fusion | flops 152322048 | bytes 1179648 | tf_op jit(solution)/shard_map/dot_general | solution.py:59
  125.5 2.9 %fusion.10 = bf16[384,512]{1,0:T(8,128)(2,1)S(1)} fusion(f32[384,512]{1,0:T(8,128)S(1)} %fusion.26, bf16[384,64,8]{0,1,2:T(8,128)(2,1)S(1)} %get-tuple-element.5), kind=kOutput, calls=%fused_computation.23 | convolution fusion | flops 152715264 | bytes 1572864 | tf_op jit(solution)/shard_map/dot_general | solution.py:59
  128.4 8.4 %convert_element_type.84 = bf16[64,384,8]{2,1,0:T(8,128)(2,1)} reshape(bf16[384,512]{1,0:T(8,128)(2,1)S(1)} %fusion.10) | data formatting | bytes 786432 | tf_op jit(solution)/shard_map/convert_element_type | solution.py:110
  136.8 5.8 %copy.38 = bf16[64,384,8]{1,2,0:T(8,128)(2,1)} copy(bf16[64,384,8]{2,1,0:T(8,128)(2,1)} %convert_element_type.84) | data formatting | bytes 786432 | tf_op jit(solution)/shard_map/convert_element_type | solution.py:110
  142.6 4.8 %all-to-all-start.2 = ((bf16[64,384,8]{1,2,0:T(8,128)(2,1)}), bf16[64,384,8]{1,2,0:T(8,128)(2,1)S(1)}, u32[]{:S(2)}, u32[]{:S(2)}) async-start(bf16[64,384,8]{1,2,0:T(8,128)(2,1)} %copy.38), calls=%async_computation.2 | async-start | bytes 786432 | tf_op jit(solution)/shard_map/all_to_all | solution.py:109
  147.4 2.5 %fusion.22 = f32[384,512]{1,0:T(8,128)S(1)} fusion(bf16[384,64,8]{0,1,2:T(8,128)(2,1)S(1)} %get-tuple-element.5), kind=kOutput, calls=%fused_computation.34 | convolution fusion | flops 152322048 | bytes 1179648 | tf_op jit(solution)/shard_map/dot_general | solution.py:59
  150.0 2.9 %fusion.11 = bf16[384,512]{1,0:T(8,128)(2,1)S(1)} fusion(f32[384,512]{1,0:T(8,128)S(1)} %fusion.22, bf16[384,64,8]{0,1,2:T(8,128)(2,1)S(1)} %get-tuple-element.6), kind=kOutput, calls=%fused_computation.24 | convolution fusion | flops 152715264 | bytes 1572864 | tf_op jit(solution)/shard_map/dot_general | solution.py:59
  152.8 8.4 %convert_element_type.87 = bf16[64,384,8]{2,1,0:T(8,128)(2,1)} reshape(bf16[384,512]{1,0:T(8,128)(2,1)S(1)} %fusion.11) | data formatting | bytes 786432 | tf_op jit(solution)/shard_map/convert_element_type | solution.py:113
  161.2 5.8 %copy.39 = bf16[64,384,8]{1,2,0:T(8,128)(2,1)} copy(bf16[64,384,8]{2,1,0:T(8,128)(2,1)} %convert_element_type.87) | data formatting | bytes 786432 | tf_op jit(solution)/shard_map/convert_element_type | solution.py:113
  167.1 12.7 %all-to-all-start.3 = ((bf16[64,384,8]{1,2,0:T(8,128)(2,1)}), bf16[64,384,8]{1,2,0:T(8,128)(2,1)S(1)}, u32[]{:S(2)}, u32[]{:S(2)}) async-start(bf16[64,384,8]{1,2,0:T(8,128)(2,1)} %copy.39), calls=%async_computation.3 | async-start | bytes 786432 | tf_op jit(solution)/shard_map/all_to_all | solution.py:112
  179.8 4.2 %fusion.16 = f32[384,512]{1,0:T(8,128)S(1)} fusion(s32[512]{0:T(512)S(1)} %get-tuple-element.11, s32[512]{0:T(512)S(1)} %get-tuple-element.12, bf16[64,384,8]{1,2,0:T(8,128)(2,1)S(1)} %all-to-all-done.2), kind=kOutput, calls=%fused_computation.27 | convolution fusion | flops 205520896 | bytes 1183744 | tf_op jit(solution)/shard_map/dot_general | solution.py:63
  184.0 10.3 %all-to-all-done.3 = bf16[64,384,8]{1,2,0:T(8,128)(2,1)S(1)} async-done(((bf16[64,384,8]{1,2,0:T(8,128)(2,1)}), bf16[64,384,8]{1,2,0:T(8,128)(2,1)S(1)}, u32[]{:S(2)}, u32[]{:S(2)}) %all-to-all-start.3) | async-done | bytes 393248 | tf_op jit(solution)/shard_map/all_to_all | solution.py:112
  194.3 7.8 %fusion.3 = bf16[1,384,2048]{2,1,0:T(8,128)(2,1)} fusion(bf16[512,2048]{0,1:T(8,128)(2,1)} %all-gather.5.cloned.1.call-done, f32[384,512]{1,0:T(8,128)S(1)} %fusion.16, s32[512]{0:T(512)S(1)} %get-tuple-element.11, s32[512]{0:T(512)S(1)} %get-tuple-element.12, bf16[64,384,8]{1,2,0:T(8,128)(2,1)S(1)} %all-to-all-done.3), kind=kOutput, calls=%fused_computation.7 | convolution fusion | flops 1012203520 | bytes 4853760 | tf_op jit(solution)/shard_map/dot_general | solution.py:118
  (14 shorter events, 0.5 us)
Async XLA Ops:
  6.5 44.8 %copy-start = (bf16[1,384,2048]{2,1,0:T(8,128)(2,1)S(1)}, bf16[1,384,2048]{2,1,0:T(8,128)(2,1)}, u32[]{:S(2)}) copy-start(bf16[1,384,2048]{2,1,0:T(8,128)(2,1)} %param.4) | copy-start | bytes 4718596
  6.5 84.8 %all-gather.7.cloned.1.call-start = ((), (), s32[]{:S(2)}) async-start(), calls=%async_computation.5 | async-start | bytes 2359296 | tf_op jit(solution)/shard_map/all_gather | solution.py:41
  50.6 133.4 %all-gather.5.cloned.1.call-start = ((), (), s32[]{:S(2)}) async-start(), calls=%async_computation.4 | async-start | bytes 2129920 | tf_op jit(solution)/shard_map/all_gather | solution.py:120
  95.2 25.3 %all-to-all-start.1 = ((bf16[384,64,8]{0,2,1:T(8,128)(2,1)}), bf16[384,64,8]{0,2,1:T(8,128)(2,1)S(1)}, u32[]{:S(2)}, u32[]{:S(2)}) async-start(bf16[384,64,8]{0,2,1:T(8,128)(2,1)} %bitcast.8), calls=%async_computation.1 | async-start | bytes 786432 | tf_op jit(solution)/shard_map/all_to_all | solution.py:88
  142.6 24.4 %all-to-all-start.2 = ((bf16[64,384,8]{1,2,0:T(8,128)(2,1)}), bf16[64,384,8]{1,2,0:T(8,128)(2,1)S(1)}, u32[]{:S(2)}, u32[]{:S(2)}) async-start(bf16[64,384,8]{1,2,0:T(8,128)(2,1)} %copy.38), calls=%async_computation.2 | async-start | bytes 786432 | tf_op jit(solution)/shard_map/all_to_all | solution.py:109
  167.1 27.3 %all-to-all-start.3 = ((bf16[64,384,8]{1,2,0:T(8,128)(2,1)}), bf16[64,384,8]{1,2,0:T(8,128)(2,1)S(1)}, u32[]{:S(2)}, u32[]{:S(2)}) async-start(bf16[64,384,8]{1,2,0:T(8,128)(2,1)} %copy.39), calls=%async_computation.3 | async-start | bytes 786432 | tf_op jit(solution)/shard_map/all_to_all | solution.py:112
Sparse Core Ops, SparseCore 0:
  50.7 40.6 all-gather.6
  94.4 85.9 all-gather.4
